TPU v7x, 32 devices: a whole 2x2x4 slice. The times are simulated.
32 devices in a mesh: grp: 2 (over y), ep: 8 (over z, x), tp: 2 (over core).
Axes of the slice: x: 2, y: 2, z: 4, core: 2. Of those that a mesh axis runs over, the one named last changes fastest.
Arguments:
- hidden_state: bfloat16 [1024, 1024], P(('grp', 'ep'), 'tp'), parts along dimension 0, may hold values from -6 to 6
- expert_ids: int32 [1024, 4], P(('grp', 'ep')), parts along dimension 0, may hold values from 0 to 7, all different within a row; in each aligned block of 64 rows (0 to 63, 64 to 127, ...) at most 64 rows name the same one
- route_weight: float32 [1024, 4], P(('grp', 'ep')), parts along dimension 0, may hold values from 0.1 to 1
- gate_matrix: bfloat16 [8, 1024, 2048], P('ep', None, 'tp'), may hold values from -0.1875 to 0.1875
- up_matrix: bfloat16 [8, 1024, 2048], P('ep', None, 'tp'), may hold values from -0.1875 to 0.1875
- down_matrix: bfloat16 [8, 2048, 1024], P('ep', 'tp'), may hold values from -2 to 2
- norm_gain: float32 [1024], P('tp'), may hold values from 0.1 to 1.9
Outputs:
- normed_out: bfloat16 [1024, 1024], P(('grp', 'ep'), 'tp'), parts along dimension 0
There are 2 independent parts, one for each index of `grp`. A program takes and returns all parts, laid end to end along the dimension named above; an argument that names none is the same for every part. Nothing has to cross between parts.
Inputs may be any that keep to these rules, and one draw needn't show every extreme that they name: `expert_ids`: each row names 4 different experts. Within the rows of one index of ep (aligned blocks of 64 rows) no expert is named by more than 64 rows, and in some blocks one expert is named by exactly 64 rows. Every expert is named by some row.
All inputs are finite; a program needn't handle non-finite values.
Results may differ from a plain program's by a relative error of at most 0.0065.
Values may be sent and summed in bfloat16 or wider, within the bound.
A program may use at most 64 MiB of HBM per device.

v0:
```python
import jax
import jax.numpy as jnp
from jax import lax
from jax.sharding import PartitionSpec as P

D = 1024


norm_eps = 1e-05


def slot_numbers(block_ids, expert_count):
    onehot = (block_ids[..., None] == jnp.arange(expert_count, dtype=jnp.int32)).astype(jnp.int32)
    earlier = jnp.cumsum(onehot, axis=-2) - onehot
    return jnp.sum(earlier * onehot, axis=-1)


def expert_rows(buffer, gate_matrix, up_matrix, down_matrix):
    sources, item_count, feature_count = buffer.shape
    token_rows = buffer.reshape(sources * item_count, feature_count)
    gate_pre = jnp.dot(token_rows, gate_matrix[0], preferred_element_type=jnp.float32)
    up_pre = jnp.dot(token_rows, up_matrix[0], preferred_element_type=jnp.float32)
    activated = (jax.nn.silu(gate_pre) * up_pre).astype(jnp.bfloat16)
    partial_value = jnp.dot(activated, down_matrix[0], preferred_element_type=jnp.float32)
    summed = lax.psum_scatter(
        partial_value.reshape(sources, item_count, feature_count).astype(jnp.bfloat16),
        "tp",
        scatter_dimension=2,
        tiled=True,
    )
    return summed


def shards(hidden_state, expert_ids, route_weight, gate_matrix, up_matrix, down_matrix, norm_gain):
    tok_count, top_count = expert_ids.shape
    expert_count = lax.axis_size("ep")
    capacity = max(2, 2 * tok_count * top_count // expert_count)
    slot_total = expert_count * capacity
    slot_rank = slot_numbers(expert_ids.reshape(1, tok_count * top_count), expert_count)
    slot_index = expert_ids * capacity + slot_rank.reshape(tok_count, top_count)
    positions = jnp.arange(slot_total, dtype=jnp.int32)
    matches = slot_index[:, :, None] == positions[None, None, :]
    placing = jnp.transpose(jnp.any(matches, axis=1)).astype(jnp.bfloat16)
    combine = jnp.sum(jnp.where(matches, route_weight[:, :, None], 0.0), axis=1)
    outgoing = jnp.dot(placing, hidden_state, preferred_element_type=jnp.float32).astype(
        jnp.bfloat16
    )
    answers = expert_rows(
        lax.all_gather(
            lax.all_to_all(
                outgoing.reshape(expert_count, capacity, hidden_state.shape[1]),
                "ep",
                split_axis=0,
                concat_axis=0,
                tiled=True,
            ),
            "tp",
            axis=2,
            tiled=True,
        ),
        gate_matrix,
        up_matrix,
        down_matrix,
    )
    returned = lax.all_to_all(answers, "ep", split_axis=0, concat_axis=0, tiled=True)
    combined = jnp.dot(
        combine,
        returned.reshape(slot_total, returned.shape[2]).astype(jnp.float32),
        precision=lax.Precision.HIGHEST,
    )
    local_squares = jnp.sum(combined * combined, axis=1)
    total_squares = lax.psum(local_squares, "tp")
    inverse_rms = lax.rsqrt(total_squares / D + norm_eps)
    return (combined * inverse_rms[:, None] * norm_gain).astype(jnp.bfloat16)


def solution(mesh):
    placed = (
        P(("grp", "ep"), "tp"),
        P(("grp", "ep"), None),
        P(("grp", "ep"), None),
        P("ep", None, "tp"),
        P("ep", None, "tp"),
        P("ep", "tp", None),
        P("tp"),
    )
    return jax.shard_map(
        shards, mesh=mesh, in_specs=placed, out_specs=P(("grp", "ep"), "tp"), check_vma=False
    )
```

profile of v0, /device:TPU:0, one launch (start us, length us, event | category | flops | bytes accessed | tf_op | source)
XLA Modules:
  0.0 88.2 jit_solution(9417557024511087397)
XLA Ops:
  6.5 0.9 %copy.18 = s32[64,4]{1,0:T(8,128)S(1)} copy(s32[64,4]{0,1:T(4,128)} %param.8) | data formatting | bytes 2048 | tf_op args[1]
  7.5 0.1 eq.40
  7.6 0.6 reduce-window.6
  8.2 0.2 slice_reduce_fusion
  8.4 0.1 fusion.13
  8.5 0.1 reshape.139
  8.6 0.1 copy.19
  8.7 0.7 multiply_add_fusion
  9.4 0.1 fusion.11
  9.5 1.2 %convolution_convert_fusion = bf16[512,512]{1,0:T(8,128)(2,1)S(1)} fusion(pred[64,512]{1,0:T(8,128)(4,1)S(1)} %fusion.11, bf16[64,512]{1,0:T(8,128)(2,1)} %param.7), kind=kOutput, calls=%fused_computation.8 | convolution fusion | flops 33816576 | bytes 622592 | tf_op jit(solution)/shard_map/dot_general | solution.py:45
  10.7 21.7 %all_to_all.10 = bf16[8,64,512]{2,1,0:T(8,128)(2,1)} all-to-all(bf16[8,64,512]{2,1,0:T(8,128)(2,1)S(1)} %bitcast.41), channel_id=1, replica_groups=mesh['grp'=2,'ep'=8,'tp'=2] {'ep'}, dimensions={0} | all-to-all | bytes 1048576 | tf_op jit(solution)/shard_map/all_to_all | solution.py:50
  32.5 0.0 reduce-scatter.2.cloned.1.call-start
  32.5 8.2 %all-gather.2.cloned.1.call-done = bf16[8,64,1024]{2,1,0:T(8,128)(2,1)} async-done(((bf16[8,64,512]{2,1,0:T(8,128)(2,1)}), bf16[8,64,1024]{2,1,0:T(8,128)(2,1)}) %all-gather.2.cloned.1.call-update) | async-done | bytes 1048592 | tf_op jit(solution)/shard_map/all_gather | solution.py:49
  40.7 2.6 %fusion.4 = f32[512,1024]{1,0:T(8,128)S(1)} fusion(bf16[512,1024]{1,0:T(8,128)(2,1)} %bitcast.43, bf16[1,1024,1024]{2,1,0:T(8,128)(2,1)S(1)} %copy-done), kind=kOutput, calls=%fused_computation.4 | convolution fusion | flops 1073741824 | bytes 5242880 | tf_op jit(solution)/shard_map/dot_general | solution.py:21
  43.4 1.4 %multiply_convert_fusion = bf16[512,1024]{1,0:T(8,128)(2,1)S(1)} fusion(f32[512,1024]{1,0:T(8,128)S(1)} %fusion.4, bf16[512,1024]{1,0:T(8,128)(2,1)S(1)} %bitcast.44, bf16[1,1024,1024]{2,1,0:T(8,128)(2,1)S(1)} %copy-done.3), kind=kOutput, calls=%fused_computation.6 | convolution fusion | flops 1076887552 | bytes 6291456 | tf_op jit(solution)/shard_map/dot_general | solution.py:22
  44.7 0.2 copy-done.4
  44.9 2.2 %fusion.8 = bf16[8,64,1024]{2,1,0:T(8,128)(2,1)} fusion(bf16[8,64,1024]{2,1,0:T(8,128)(2,1)S(1)} %bitcast.45, bf16[1,1024,1024]{2,1,0:T(8,128)(2,1)S(1)} %copy-done.4), kind=kOutput, calls=%fused_computation.7 | convolution fusion | flops 1074266112 | bytes 4194304 | tf_op jit(solution)/shard_map/dot_general | solution.py:24
  47.2 9.7 %reduce-scatter.2.cloned.1.call-done = bf16[8,64,512]{2,1,0:T(8,128)(2,1)} async-done(((bf16[8,64,1024]{2,1,0:T(8,128)(2,1)}), bf16[8,64,512]{2,1,0:T(8,128)(2,1)}) %reduce-scatter.2.cloned.1.call-update) | async-done | bytes 524304 | tf_op jit(solution)/shard_map/reduce_scatter | solution.py:25
  56.9 5.8 %all-to-all-start.1 = ((bf16[8,64,512]{2,1,0:T(8,128)(2,1)}), bf16[8,64,512]{2,1,0:T(8,128)(2,1)S(1)}, u32[]{:S(2)}, u32[]{:S(2)}) async-start(bf16[8,64,512]{2,1,0:T(8,128)(2,1)} %reduce-scatter.2.cloned.1.call-done), calls=%async_computation.2 | async-start | bytes 1048576 | tf_op jit(solution)/shard_map/all_to_all | solution.py:65
  62.7 0.1 select_reduce_fusion
  62.8 14.8 %all-to-all-done.1 = bf16[8,64,512]{2,1,0:T(8,128)(2,1)S(1)} async-done(((bf16[8,64,512]{2,1,0:T(8,128)(2,1)}), bf16[8,64,512]{2,1,0:T(8,128)(2,1)S(1)}, u32[]{:S(2)}, u32[]{:S(2)}) %all-to-all-start.1) | async-done | bytes 524320 | tf_op jit(solution)/shard_map/all_to_all | solution.py:65
  77.6 0.5 multiply_reduce_fusion
  78.1 2.5 %psum.7 = f32[64]{0:T(128)S(1)} all-reduce(f32[64]{0:T(128)S(1)} %get-tuple-element.5), channel_id=1, replica_groups=mesh['grp'=2,'ep'=8,'tp'=2] {'tp'}, use_global_device_ids=true, to_apply=%region_7.8 | all-reduce | flops 64 | bytes 512 | tf_op jit(solution)/shard_map/psum | solution.py:72
  80.6 0.7 multiply_convert_fusion.1
  (18 shorter events, 0.1 us)
Async XLA Ops:
  6.5 34.2 %copy-start = (bf16[1,1024,1024]{2,1,0:T(8,128)(2,1)S(1)}, bf16[1,1024,1024]{2,1,0:T(8,128)(2,1)}, u32[]{:S(2)}) copy-start(bf16[1,1024,1024]{2,1,0:T(8,128)(2,1)} %param.10) | copy-start | bytes 6291460
  6.5 34.2 %all-gather.2.cloned.1.call-start = ((), (), s32[]{:S(2)}) async-start(), calls=%async_computation.3 | async-start | bytes 1572864 | tf_op jit(solution)/shard_map/all_gather | solution.py:49
  32.5 24.4 %reduce-scatter.2.cloned.1.call-start = ((), (), s32[]{:S(2)}) async-start(), calls=%async_computation.4 | async-start | bytes 1572864 | tf_op jit(solution)/shard_map/reduce_scatter | solution.py:25
  40.7 2.6 %copy-start.3 = (bf16[1,1024,1024]{2,1,0:T(8,128)(2,1)S(1)}, bf16[1,1024,1024]{2,1,0:T(8,128)(2,1)}, u32[]{:S(2)}) copy-start(bf16[1,1024,1024]{2,1,0:T(8,128)(2,1)} %param.11) | copy-start | bytes 6291460
  40.7 2.6 %copy-start.5 = (bf16[8,64,1024]{2,1,0:T(8,128)(2,1)S(1)}, bf16[8,64,1024]{2,1,0:T(8,128)(2,1)}, u32[]{:S(2)}) copy-start(bf16[8,64,1024]{2,1,0:T(8,128)(2,1)} %all-gather.2.cloned.1.call-done) | copy-start | bytes 3145732
  43.3 1.6 %copy-start.4 = (bf16[1,1024,1024]{2,1,0:T(8,128)(2,1)S(1)}, bf16[1,1024,1024]{2,1,0:T(8,128)(2,1)}, u32[]{:S(2)}) copy-start(bf16[1,1024,1024]{2,1,0:T(8,128)(2,1)} %param.12) | copy-start | bytes 6291460
  47.2 15.5 %copy-start.1 = (f32[64,4]{0,1:T(4,128)S(1)}, f32[64,4]{0,1:T(4,128)}, u32[]{:S(2)}) copy-start(f32[64,4]{0,1:T(4,128)} %param.9) | copy-start | bytes 3076
  47.2 33.4 %copy-start.2 = (f32[512]{0:T(512)S(1)}, f32[512]{0:T(512)}, u32[]{:S(2)}) copy-start(f32[512]{0:T(512)} %param.13) | copy-start | bytes 6148
  56.9 20.7 %all-to-all-start.1 = ((bf16[8,64,512]{2,1,0:T(8,128)(2,1)}), bf16[8,64,512]{2,1,0:T(8,128)(2,1)S(1)}, u32[]{:S(2)}, u32[]{:S(2)}) async-start(bf16[8,64,512]{2,1,0:T(8,128)(2,1)} %reduce-scatter.2.cloned.1.call-done), calls=%async_computation.2 | async-start | bytes 1048576 | tf_op jit(solution)/shard_map/all_to_all | solution.py:65
Sparse Core Ops, SparseCore 0:
  32.6 8.0 all-gather.1
  47.3 9.5 reduce-scatter.1
where the time goes:
time: 88.5 us; the launch traced here: 88.2 us
  waiting for transfers between devices  32.7 us (37%)
  blocking collectives  24.2 us (27%)
  between operations  13.5 us (15%)
  matrix products  7.91 us (9%)
  starting transfers between devices  5.82 us (7%)
  other arithmetic  2.42 us (3%)
  local copies, waits for them, and re-layouts  1.65 us (2%)
    all_to_all x1, blocking collectives, shards(): lax.all_to_all(outgoing.reshape(expert_count, capacity, hidden_state.shap...  21.7 us
    all_to_all x1, waiting for transfers between devices, shards(): lax.all_to_all(answers, 'ep', split_axis=0, concat_axis=0, tiled=True)  14.8 us
    reduce_scatter x1, waiting for transfers between devices, expert_rows(): lax.psum_scatter(partial_value.reshape(sources, item_count, feature_count...  9.7 us
    all_gather x1, waiting for transfers between devices, shards(): lax.all_gather(lax.all_to_all(outgoing.reshape(expert_count, capacity, hi...  8.17 us
    all_to_all x1, starting transfers between devices, shards(): lax.all_to_all(answers, 'ep', split_axis=0, concat_axis=0, tiled=True)  5.78 us
    dot_general x1, matrix products, expert_rows(): jnp.dot(token_rows, gate_matrix[0], preferred_element_type=jnp.float32)  2.62 us
    psum x1, blocking collectives, shards(): total_squares = lax.psum(local_squares, 'tp')  2.47 us
    dot_general x1, matrix products, expert_rows(): jnp.dot(activated, down_matrix[0], preferred_element_type=jnp.float32)  2.24 us
  transfers between devices with their start and end apart: 3, of which 3 were waited for; matrix products, arithmetic and copies ran while one was open for 0% of the time, Pallas kernels for 0%

commit v1 on v0

--- a/solution.py
+++ b/solution.py
@@ -1,11 +1,13 @@
+import functools
+
 import jax
 import jax.numpy as jnp
 from jax import lax
+from jax.experimental import pallas as pl
+from jax.experimental.pallas import tpu as pltpu
 from jax.sharding import PartitionSpec as P
 
-D = 1024
-
-
+MESH = pl.DeviceIdType.MESH
 norm_eps = 1e-05
 
 
@@ -22,18 +24,18 @@
     up_pre = jnp.dot(token_rows, up_matrix[0], preferred_element_type=jnp.float32)
     activated = (jax.nn.silu(gate_pre) * up_pre).astype(jnp.bfloat16)
     partial_value = jnp.dot(activated, down_matrix[0], preferred_element_type=jnp.float32)
-    summed = lax.psum_scatter(
+    return lax.psum_scatter(
         partial_value.reshape(sources, item_count, feature_count).astype(jnp.bfloat16),
         "tp",
         scatter_dimension=2,
         tiled=True,
     )
-    return summed
-
-
-def shards(hidden_state, expert_ids, route_weight, gate_matrix, up_matrix, down_matrix, norm_gain):
+
+
+def slotted(hidden_state, expert_ids, route_weight, gate_matrix, up_matrix, down_matrix, norm_gain):
     tok_count, top_count = expert_ids.shape
     expert_count = lax.axis_size("ep")
+    feature_total = hidden_state.shape[1] * lax.axis_size("tp")
     capacity = max(2, 2 * tok_count * top_count // expert_count)
     slot_total = expert_count * capacity
     slot_rank = slot_numbers(expert_ids.reshape(1, tok_count * top_count), expert_count)
@@ -45,22 +47,15 @@
     outgoing = jnp.dot(placing, hidden_state, preferred_element_type=jnp.float32).astype(
         jnp.bfloat16
     )
+    received = lax.all_to_all(
+        outgoing.reshape(expert_count, capacity, hidden_state.shape[1]),
+        "ep",
+        split_axis=0,
+        concat_axis=0,
+        tiled=True,
+    )
     answers = expert_rows(
-        lax.all_gather(
-            lax.all_to_all(
-                outgoing.reshape(expert_count, capacity, hidden_state.shape[1]),
-                "ep",
-                split_axis=0,
-                concat_axis=0,
-                tiled=True,
-            ),
-            "tp",
-            axis=2,
-            tiled=True,
-        ),
-        gate_matrix,
-        up_matrix,
-        down_matrix,
+        lax.all_gather(received, "tp", axis=2, tiled=True), gate_matrix, up_matrix, down_matrix
     )
     returned = lax.all_to_all(answers, "ep", split_axis=0, concat_axis=0, tiled=True)
     combined = jnp.dot(
@@ -68,10 +63,200 @@
         returned.reshape(slot_total, returned.shape[2]).astype(jnp.float32),
         precision=lax.Precision.HIGHEST,
     )
-    local_squares = jnp.sum(combined * combined, axis=1)
-    total_squares = lax.psum(local_squares, "tp")
-    inverse_rms = lax.rsqrt(total_squares / D + norm_eps)
+    total_squares = lax.psum(jnp.sum(combined * combined, axis=1), "tp")
+    inverse_rms = lax.rsqrt(total_squares / feature_total + norm_eps)
     return (combined * inverse_rms[:, None] * norm_gain).astype(jnp.bfloat16)
+
+
+def kernel(
+    nz, nx, ids, rw, h, g_hbm, u_hbm, d_hbm, gain, out,
+    xs, gw, uw, dw, act, psend, precv, ys, ret, sq, sqr,
+    wsem, osem, gs, gr, ps, pr, ds, dr, rs, rr, qs, qr,
+):
+    n = nz * nx
+    tok, half = h.shape
+    rows = nz * tok
+    me = lax.axis_index("ep")
+    z, x = me // nx, me % nx
+    c = lax.axis_index("tp")
+    other = (c + 1) % 2
+    mine = x * nz + z
+
+    weights = [
+        pltpu.make_async_copy(g_hbm.at[0], gw, wsem.at[0]),
+        pltpu.make_async_copy(u_hbm.at[0], uw, wsem.at[1]),
+        pltpu.make_async_copy(d_hbm.at[0], dw, wsem.at[2]),
+    ]
+    own = pltpu.make_async_copy(h, xs.at[c, mine], osem)
+    own.start()
+    for w in weights:
+        w.start()
+
+    barrier = pltpu.get_barrier_semaphore()
+    for k in range(1, n):
+        pl.semaphore_signal(
+            barrier, inc=1, device_id={"ep": (me + k) % n}, device_id_type=MESH
+        )
+    pl.semaphore_signal(barrier, inc=1, device_id={"tp": other}, device_id_type=MESH)
+    pl.semaphore_wait(barrier, n)
+
+    def place(j, dz):
+        zz, xx = (z + dz) % nz, (x + j) % nx
+        return zz * nx + xx, xx * nz + zz
+
+    def to_chip(src, dst, send, recv, chip):
+        return pltpu.make_async_remote_copy(
+            src_ref=src, dst_ref=dst, send_sem=send, recv_sem=recv,
+            device_id={"ep": chip}, device_id_type=MESH,
+        )
+
+    def to_core(src, dst, send, recv):
+        return pltpu.make_async_remote_copy(
+            src_ref=src, dst_ref=dst, send_sem=send, recv_sem=recv,
+            device_id={"tp": other}, device_id_type=MESH,
+        )
+
+    order = [(j, dz) for j in range(nx) for dz in range(nz)]
+    started = []
+    for j, dz in order[1:]:
+        chip, slot = place(j, dz)
+        copy = to_chip(h, xs.at[c, mine], gs.at[slot], gr.at[mine], chip)
+        copy.start()
+        started.append(copy)
+    first = to_core(h, xs.at[c, mine], ps.at[mine], pr.at[mine])
+    first.start()
+    started.append(first)
+    own.wait()
+
+    def waited(ref, send, recv):
+        return to_core(ref, ref, send, recv)
+
+    for j in range(nx):
+        col = (x + j) % nx
+        for dz in range(nz):
+            if (j, dz) == (0, 0):
+                continue
+            chip, slot = place(j, dz)
+            waited(xs.at[c, slot], gs.at[slot], gr.at[slot]).wait_recv()
+            copy = to_core(xs.at[c, slot], xs.at[c, slot], ps.at[slot], pr.at[slot])
+            copy.start()
+            started.append(copy)
+        for dz in range(nz):
+            chip, slot = place(j, dz)
+            waited(xs.at[other, slot], ps.at[slot], pr.at[slot]).wait_recv()
+        if j == 0:
+            weights[0].wait()
+            weights[1].wait()
+        low = xs[0, pl.ds(col * nz, nz)].reshape(rows, half)
+        high = xs[1, pl.ds(col * nz, nz)].reshape(rows, half)
+        hid = gw.shape[1]
+        tile = min(256, hid)
+        for at in range(0, hid, tile):
+            cut = slice(at, at + tile)
+            gate = jnp.dot(low, gw[:half, cut], preferred_element_type=jnp.float32)
+            gate += jnp.dot(high, gw[half:, cut], preferred_element_type=jnp.float32)
+            up = jnp.dot(low, uw[:half, cut], preferred_element_type=jnp.float32)
+            up += jnp.dot(high, uw[half:, cut], preferred_element_type=jnp.float32)
+            act[:, cut] = (jax.nn.silu(gate) * up).astype(jnp.bfloat16)
+        if j == 0:
+            weights[2].wait()
+        theirs = pl.ds(pl.multiple_of(other * half, half), half)
+        ours = pl.ds(pl.multiple_of(c * half, half), half)
+        psend[j] = jnp.dot(
+            act[...], dw[:, theirs], preferred_element_type=jnp.float32
+        ).astype(jnp.bfloat16)
+        swap = to_core(psend.at[j], precv.at[j], ds.at[j], dr.at[j])
+        swap.start()
+        part = jnp.dot(act[...], dw[:, ours], preferred_element_type=jnp.float32).astype(
+            jnp.bfloat16
+        )
+        swap.wait()
+        total = (part.astype(jnp.float32) + precv[j].astype(jnp.float32)).astype(jnp.bfloat16)
+        ys[pl.ds(col * nz, nz)] = total.reshape(nz, tok, half)
+        for dz in range(nz):
+            if (j, dz) == (0, 0):
+                continue
+            chip, slot = place(j, dz)
+            copy = to_chip(ys.at[slot], ret.at[mine], rs.at[slot], rr.at[mine], chip)
+            copy.start()
+            started.append(copy)
+
+    total = None
+    for j, dz in order:
+        chip, slot = place(j, dz)
+        weight = jnp.zeros((tok, 1), jnp.float32)
+        for k in range(ids.shape[1]):
+            weight += jnp.where(ids[:, k : k + 1] == chip, rw[:, k : k + 1], 0.0)
+        if (j, dz) == (0, 0):
+            block = ys[mine]
+        else:
+            waited(ret.at[slot], rs.at[slot], rr.at[slot]).wait_recv()
+            block = ret[slot]
+        term = weight * block.astype(jnp.float32)
+        total = term if total is None else total + term
+    squares = jnp.sum(total * total, axis=1, keepdims=True)
+    sq[...] = jnp.broadcast_to(squares, sq.shape)
+    share = to_core(sq, sqr, qs, qr)
+    share.start()
+    share.wait()
+    mean = (squares + sqr[:, :1]) / (half * 2)
+    out[...] = (total * lax.rsqrt(mean + norm_eps) * gain[...]).astype(jnp.bfloat16)
+    for copy in started:
+        copy.wait_send()
+
+
+def shards(hidden_state, expert_ids, route_weight, gate_matrix, up_matrix, down_matrix, norm_gain):
+    tok, top = expert_ids.shape
+    half = hidden_state.shape[1]
+    hid = gate_matrix.shape[2]
+    n = lax.axis_size("ep")
+    if 2 * tok * top // n < tok or lax.axis_size("tp") != 2 or n % 2:
+        return slotted(
+            hidden_state, expert_ids, route_weight, gate_matrix, up_matrix, down_matrix, norm_gain
+        )
+    nx = 2
+    nz = n // nx
+    bf16, f32 = jnp.bfloat16, jnp.float32
+    vmem = pl.BlockSpec(memory_space=pltpu.VMEM)
+    hbm = pl.BlockSpec(memory_space=pl.ANY)
+    dma = pltpu.SemaphoreType.DMA
+    return pl.pallas_call(
+        functools.partial(kernel, nz, nx),
+        out_shape=jax.ShapeDtypeStruct((tok, half), bf16),
+        in_specs=[vmem, vmem, vmem, hbm, hbm, hbm, vmem],
+        out_specs=vmem,
+        scratch_shapes=[
+            pltpu.VMEM((2, n, tok, half), bf16),
+            pltpu.VMEM((2 * half, hid), bf16),
+            pltpu.VMEM((2 * half, hid), bf16),
+            pltpu.VMEM((hid, 2 * half), bf16),
+            pltpu.VMEM((nz * tok, hid), bf16),
+            pltpu.VMEM((nx, nz * tok, half), bf16),
+            pltpu.VMEM((nx, nz * tok, half), bf16),
+            pltpu.VMEM((n, tok, half), bf16),
+            pltpu.VMEM((n, tok, half), bf16),
+            pltpu.VMEM((tok, 128), f32),
+            pltpu.VMEM((tok, 128), f32),
+            dma((3,)),
+            dma,
+            dma((n,)),
+            dma((n,)),
+            dma((n,)),
+            dma((n,)),
+            dma((nx,)),
+            dma((nx,)),
+            dma((n,)),
+            dma((n,)),
+            dma,
+            dma,
+        ],
+        compiler_params=pltpu.CompilerParams(
+            collective_id=0, has_side_effects=True, vmem_limit_bytes=48 * 1024 * 1024
+        ),
+    )(
+        expert_ids, route_weight, hidden_state, gate_matrix, up_matrix, down_matrix,
+        norm_gain.reshape(1, half),
+    )
 
 
 def solution(mesh):

time: 88.5 us -> 40 us (0.45)
  waiting for transfers between devices: 32.7 us -> 0 us
  Pallas kernels: 0 us -> 32.3 us
  blocking collectives: 24.2 us -> 0 us
  between operations: 13.5 us -> 0.01 us
  matrix products: 7.91 us -> 0 us
  starting transfers between devices: 5.82 us -> 0 us
  local copies, waits for them, and re-layouts: 1.65 us -> 6.87 us
  other arithmetic: 2.42 us -> 0 us
    pallas_call x0 -> x1, Pallas kernels: none -> 32.3 us  [shards(): pl.pallas_call(functools.partial(kernel, nz, nx), out_shape=jax.ShapeDtyp...]
    all_to_all x1 -> x0, blocking collectives: 21.7 us -> none  [shards(): lax.all_to_all(outgoing.reshape(expert_count, capacity, hidden_state.shap...]
    all_to_all x1 -> x0, waiting for transfers between devices: 14.8 us -> none  [shards(): lax.all_to_all(answers, 'ep', split_axis=0, concat_axis=0, tiled=True)]
    reduce_scatter x1 -> x0, waiting for transfers between devices: 9.7 us -> none  [expert_rows(): lax.psum_scatter(partial_value.reshape(sources, item_count, feature_count...]
    all_gather x1 -> x0, waiting for transfers between devices: 8.17 us -> none  [shards(): lax.all_gather(lax.all_to_all(outgoing.reshape(expert_count, capacity, hi...]
    dot_general x5 -> x0, matrix products: 7.91 us -> none  [the longest x1 2.62 us: expert_rows(): jnp.dot(token_rows, gate_matrix[0], preferred_element_type=jnp.float32)]
    all_to_all x1 -> x0, starting transfers between devices: 5.78 us -> none  [shards(): lax.all_to_all(answers, 'ep', split_axis=0, concat_axis=0, tiled=True)]
    unnamed x13 -> x11, local copies, waits for them, and re-layouts: 1.15 us -> 6.87 us
  transfers between devices with their start and end apart: 3 -> 0, of which waited for: 3 -> 0; matrix products, arithmetic and copies ran while one was open for 0% -> 0% of each run, Pallas kernels for 0% -> 0%
where the time goes in v1:
time: 40 us; the launch traced here: 39.2 us
  Pallas kernels  32.3 us (81%)
  local copies, waits for them, and re-layouts  6.87 us (17%)
    pallas_call x1, Pallas kernels, shards(): pl.pallas_call(functools.partial(kernel, nz, nx), out_shape=jax.ShapeDtyp...  32.3 us
    unnamed x11, local copies, waits for them, and re-layouts  6.87 us

profile of v1, /device:TPU:0, one launch (start us, length us, event | category | flops | bytes accessed | tf_op | source)
XLA Modules:
  0.0 39.2 jit_solution(11041611119045424325)
XLA Ops:
  0.0 0.8 %copy.8.ids = s32[64,4]{1,0:T(8,128)S(1)} copy(s32[64,4]{0,1:T(4,128)} %param.8) | data formatting | bytes 2048 | tf_op args[1]
  0.8 0.8 %copy.9.rw = f32[64,4]{1,0:T(8,128)S(1)} copy(f32[64,4]{0,1:T(4,128)} %param.9) | data formatting | bytes 2048 | tf_op args[2]
  1.5 0.0 copy-start
  1.5 1.6 %copy-done = bf16[1,1024,1024]{2,1,0:T(8,128)(2,1)S(1)} copy-done((bf16[1,1024,1024]{2,1,0:T(8,128)(2,1)S(1)}, bf16[1,1024,1024]{2,1,0:T(8,128)(2,1)}, u32[]{:S(2)}) %copy-start) | copy-done | bytes 2097176
  3.1 0.0 copy-start.1
  3.1 1.6 %copy-done.1 = bf16[1,1024,1024]{2,1,0:T(8,128)(2,1)S(1)} copy-done((bf16[1,1024,1024]{2,1,0:T(8,128)(2,1)S(1)}, bf16[1,1024,1024]{2,1,0:T(8,128)(2,1)}, u32[]{:S(2)}) %copy-start.1) | copy-done | bytes 2097176
  4.7 0.0 copy-start.2
  4.7 0.8 %copy-done.2 = bf16[64,512]{1,0:T(8,128)(2,1)S(1)} copy-done((bf16[64,512]{1,0:T(8,128)(2,1)S(1)}, bf16[64,512]{1,0:T(8,128)(2,1)}, u32[]{:S(2)}) %copy-start.2) | copy-done | bytes 65560
  5.6 0.0 copy-start.3
  5.6 0.7 %copy-done.3 = f32[512]{0:T(512)S(1)} copy-done((f32[512]{0:T(512)S(1)}, f32[512]{0:T(512)}, u32[]{:S(2)}) %copy-start.3) | copy-done | bytes 2072
  6.2 32.3 %shard_map.73 = bf16[64,512]{1,0:T(8,128)(2,1)S(1)} custom-call(s32[64,4]{1,0:T(8,128)S(1)} %copy.8.ids, f32[64,4]{1,0:T(8,128)S(1)} %copy.9.rw, bf16[64,512]{1,0:T(8,128)(2,1)S(1)} %copy-done.2, bf16[1,1024,1024]{2,1,0:T(8,128)(2,1)S(1)} %copy-done, bf16[1,1024,1024]{2,1,0:T(8,128)(2,1)S(1)} %copy-done.1, bf16[1,1024,1024]{2,1,0:T(8,128)(2,1)} %d_hbm.1, ...), custom_call_target="tpu_custom_call" | custom-call | tf_op jit(solution)/shard_map/pallas_call | solution.py:223
  38.6 0.6 %copy.11 = bf16[64,512]{1,0:T(8,128)(2,1)} copy(bf16[64,512]{1,0:T(8,128)(2,1)S(1)} %shard_map.73) | data formatting | bytes 131072
Async XLA Ops:
  1.5 1.6 %copy-start = (bf16[1,1024,1024]{2,1,0:T(8,128)(2,1)S(1)}, bf16[1,1024,1024]{2,1,0:T(8,128)(2,1)}, u32[]{:S(2)}) copy-start(bf16[1,1024,1024]{2,1,0:T(8,128)(2,1)} %g_hbm.1) | copy-start | bytes 6291460
  3.1 1.6 %copy-start.1 = (bf16[1,1024,1024]{2,1,0:T(8,128)(2,1)S(1)}, bf16[1,1024,1024]{2,1,0:T(8,128)(2,1)}, u32[]{:S(2)}) copy-start(bf16[1,1024,1024]{2,1,0:T(8,128)(2,1)} %u_hbm.1) | copy-start | bytes 6291460
  4.7 0.8 %copy-start.2 = (bf16[64,512]{1,0:T(8,128)(2,1)S(1)}, bf16[64,512]{1,0:T(8,128)(2,1)}, u32[]{:S(2)}) copy-start(bf16[64,512]{1,0:T(8,128)(2,1)} %h.1) | copy-start | bytes 196612
  5.6 0.7 %copy-start.3 = (f32[512]{0:T(512)S(1)}, f32[512]{0:T(512)}, u32[]{:S(2)}) copy-start(f32[512]{0:T(512)} %param.13) | copy-start | bytes 6148

commit v2 on v1

v2 whole, which is shorter than its diff:
```python
import functools

import jax
import jax.numpy as jnp
from jax import lax
from jax.experimental import pallas as pl
from jax.experimental.pallas import tpu as pltpu
from jax.sharding import PartitionSpec as P

MESH = pl.DeviceIdType.MESH
norm_eps = 1e-05


def slot_numbers(block_ids, expert_count):
    onehot = (block_ids[..., None] == jnp.arange(expert_count, dtype=jnp.int32)).astype(jnp.int32)
    earlier = jnp.cumsum(onehot, axis=-2) - onehot
    return jnp.sum(earlier * onehot, axis=-1)


def expert_rows(buffer, gate_matrix, up_matrix, down_matrix):
    sources, item_count, feature_count = buffer.shape
    token_rows = buffer.reshape(sources * item_count, feature_count)
    gate_pre = jnp.dot(token_rows, gate_matrix[0], preferred_element_type=jnp.float32)
    up_pre = jnp.dot(token_rows, up_matrix[0], preferred_element_type=jnp.float32)
    activated = (jax.nn.silu(gate_pre) * up_pre).astype(jnp.bfloat16)
    partial_value = jnp.dot(activated, down_matrix[0], preferred_element_type=jnp.float32)
    return lax.psum_scatter(
        partial_value.reshape(sources, item_count, feature_count).astype(jnp.bfloat16),
        "tp",
        scatter_dimension=2,
        tiled=True,
    )


def slotted(hidden_state, expert_ids, route_weight, gate_matrix, up_matrix, down_matrix, norm_gain):
    tok_count, top_count = expert_ids.shape
    expert_count = lax.axis_size("ep")
    feature_total = hidden_state.shape[1] * lax.axis_size("tp")
    capacity = max(2, 2 * tok_count * top_count // expert_count)
    slot_total = expert_count * capacity
    slot_rank = slot_numbers(expert_ids.reshape(1, tok_count * top_count), expert_count)
    slot_index = expert_ids * capacity + slot_rank.reshape(tok_count, top_count)
    positions = jnp.arange(slot_total, dtype=jnp.int32)
    matches = slot_index[:, :, None] == positions[None, None, :]
    placing = jnp.transpose(jnp.any(matches, axis=1)).astype(jnp.bfloat16)
    combine = jnp.sum(jnp.where(matches, route_weight[:, :, None], 0.0), axis=1)
    outgoing = jnp.dot(placing, hidden_state, preferred_element_type=jnp.float32).astype(
        jnp.bfloat16
    )
    received = lax.all_to_all(
        outgoing.reshape(expert_count, capacity, hidden_state.shape[1]),
        "ep",
        split_axis=0,
        concat_axis=0,
        tiled=True,
    )
    answers = expert_rows(
        lax.all_gather(received, "tp", axis=2, tiled=True), gate_matrix, up_matrix, down_matrix
    )
    returned = lax.all_to_all(answers, "ep", split_axis=0, concat_axis=0, tiled=True)
    combined = jnp.dot(
        combine,
        returned.reshape(slot_total, returned.shape[2]).astype(jnp.float32),
        precision=lax.Precision.HIGHEST,
    )
    total_squares = lax.psum(jnp.sum(combined * combined, axis=1), "tp")
    inverse_rms = lax.rsqrt(total_squares / feature_total + norm_eps)
    return (combined * inverse_rms[:, None] * norm_gain).astype(jnp.bfloat16)


def kernel(
    nz, nx, ids_hbm, rw_hbm, h_hbm, g_hbm, u_hbm, d_hbm, gain_hbm, out,
    ids, rw, gain, xs, gw, uw, dw, act, psend, precv, acc, ys, yx, zs, ret, sq, sqr,
    wsem, osem, gs, gr, fs, ps, pr, ns, nr, ds, dr, us, ur, rs, rr, qs, qr,
):
    tok, half = out.shape
    hid = gw.shape[1]
    pairs = nz // 2
    me = lax.axis_index("ep")
    z, x = me // nx, me % nx
    beside = (x + 1) % nx
    c = lax.axis_index("tp")
    other = (c + 1) % 2
    mine = x * nz + z

    def local(src, dst, sem):
        copy = pltpu.make_async_copy(src, dst, sem)
        copy.start()
        return copy

    own = local(h_hbm, xs.at[c, mine], osem.at[0])
    own_ids = local(ids_hbm, ids.at[z], osem.at[1])
    own_rw = local(rw_hbm, rw.at[z], osem.at[2])
    weights = [
        local(g_hbm.at[0], gw, wsem.at[0]),
        local(u_hbm.at[0], uw, wsem.at[1]),
        local(d_hbm.at[0], dw, wsem.at[2]),
    ]
    own_gain = local(gain_hbm, gain, osem.at[3])

    def row_of(d, r):
        return 2 * ((z // 2 + d) % pairs) + (z + r) % 2

    def far(d, r):
        return (d, r) != (0, 0)

    spots = [(d, r) for d in range(pairs) for r in (1, 0)]
    peers = [spot for spot in spots if far(*spot)]

    barrier = pltpu.get_barrier_semaphore()
    for d, r in peers:
        pl.semaphore_signal(
            barrier, inc=1, device_id={"ep": row_of(d, r) * nx + x}, device_id_type=MESH
        )
    pl.semaphore_signal(
        barrier, inc=1, device_id={"ep": z * nx + beside}, device_id_type=MESH
    )
    pl.semaphore_signal(barrier, inc=1, device_id={"tp": other}, device_id_type=MESH)
    own.wait()
    own_ids.wait()
    own_rw.wait()
    pl.semaphore_wait(barrier, nz + 1)

    def remote(src, dst, send, recv, where):
        return pltpu.make_async_remote_copy(
            src_ref=src, dst_ref=dst, send_sem=send, recv_sem=recv,
            device_id=where, device_id_type=MESH,
        )

    def along(row):
        return {"ep": row * nx + x}

    across = {"ep": z * nx + beside}
    twin = {"tp": other}
    started = []

    def send(*what):
        copy = remote(*what)
        copy.start()
        started.append(copy)
        return copy

    block = xs.at[c, mine]
    send(block, block, fs.at[z], gr.at[mine], across)
    for d, r in peers:
        row = row_of(d, r)
        send(block, block, gs.at[row], gr.at[mine], along(row))
    send(block, block, ps.at[mine], pr.at[mine], twin)
    for d, r in peers:
        row = row_of(d, r)
        send(ids.at[z], ids.at[z], ns.at[0, row], nr.at[0, z], along(row))
        send(rw.at[z], rw.at[z], ns.at[1, row], nr.at[1, z], along(row))

    def arrive(j, d, r):
        if j == 0 and not far(d, r):
            return
        row = row_of(d, r)
        slot = (x + j) % nx * nz + row
        ref = xs.at[c, slot]
        remote(ref, ref, ps.at[slot], gr.at[slot], twin).wait_recv()
        if j == 0:
            send(ref, ref, fs.at[row], gr.at[slot], across)
        send(ref, ref, ps.at[slot], pr.at[slot], twin)

    theirs = pl.ds(pl.multiple_of(other * half, half), half)
    ours = pl.ds(pl.multiple_of(c * half, half), half)
    kept = {}

    def compute(j, d):
        for r in range(2):
            slot = (x + j) % nx * nz + row_of(d, r)
            ref = xs.at[other, slot]
            remote(ref, ref, ps.at[slot], pr.at[slot], twin).wait_recv()
        if (j, d) == (0, 0):
            weights[0].wait()
            weights[1].wait()
        base = (x + j) % nx * nz + 2 * ((z // 2 + d) % pairs)
        low = xs[0, pl.ds(base, 2)].reshape(2 * tok, half)
        high = xs[1, pl.ds(base, 2)].reshape(2 * tok, half)
        tile = min(256, hid)
        for at in range(0, hid, tile):
            cut = slice(at, at + tile)
            gate = jnp.dot(low, gw[:half, cut], preferred_element_type=jnp.float32)
            gate += jnp.dot(high, gw[half:, cut], preferred_element_type=jnp.float32)
            up = jnp.dot(low, uw[:half, cut], preferred_element_type=jnp.float32)
            up += jnp.dot(high, uw[half:, cut], preferred_element_type=jnp.float32)
            act[:, cut] = (jax.nn.silu(gate) * up).astype(jnp.bfloat16)
        if (j, d) == (0, 0):
            weights[2].wait()
        q = 2 * d + j
        psend[q] = jnp.dot(
            act[...], dw[:, theirs], preferred_element_type=jnp.float32
        ).astype(jnp.bfloat16)
        swap = remote(psend.at[q], precv.at[q], ds.at[q], dr.at[q], twin)
        swap.start()
        kept[q] = swap
        part = jnp.dot(act[...], dw[:, ours], preferred_element_type=jnp.float32)
        part = part.astype(jnp.bfloat16).reshape(2, tok, half)
        lower = 2 * ((z // 2 + d) % pairs)
        if j == 0:
            acc[pl.ds(lower, 2)] = part.astype(jnp.float32)
        else:
            ys[pl.ds(lower, 2)] = part

    eye = lax.broadcasted_iota(jnp.int32, (tok, tok), 0) == lax.broadcasted_iota(
        jnp.int32, (tok, tok), 1
    )

    def weight_of(row, chip):
        line = jnp.zeros((1, tok), jnp.float32)
        for k in range(ids.shape[1]):
            line += jnp.where(ids[row, k : k + 1] == chip, rw[row, k : k + 1], 0.0)
        return jnp.sum(jnp.where(eye, line, 0.0), axis=1, keepdims=True)

    def keep(d):
        q = 2 * d
        kept[q].wait()
        for r in range(2):
            row = row_of(d, r)
            if far(d, r):
                for i, ref in enumerate((ids, rw)):
                    remote(
                        ref.at[row], ref.at[row], ns.at[i, row], nr.at[i, row], along(row)
                    ).wait_recv()
            got = precv[q, pl.ds(pl.multiple_of(row % 2 * tok, tok), tok)]
            done = (acc[row] + got.astype(jnp.float32)).astype(jnp.bfloat16)
            acc[row] = done.astype(jnp.float32) * weight_of(row, me)

    def pass_on(d):
        q = 2 * d + 1
        kept[q].wait()
        for r in (1, 0):
            row = row_of(d, r)
            got = precv[q, pl.ds(pl.multiple_of(row % 2 * tok, tok), tok)]
            done = ys[row].astype(jnp.float32) + got.astype(jnp.float32)
            ys[row] = done.astype(jnp.bfloat16)
            send(ys.at[row], yx.at[row], us.at[row], ur.at[row], across)

    def relay(d):
        for r in (1, 0):
            row = row_of(d, r)
            weight = weight_of(row, z * nx + beside)
            remote(yx.at[row], yx.at[row], us.at[row], ur.at[row], across).wait_recv()
            both = acc[row] + weight * yx[row].astype(jnp.float32)
            if far(d, r):
                zs[row] = both.astype(jnp.bfloat16)
                send(zs.at[row], ret.at[z], rs.at[row], rr.at[z], along(row))
            else:
                acc[row] = both

    arrive(0, 0, 1)
    for d in range(pairs):
        if d > 0:
            arrive(0, d, 0)
        compute(0, d)
        arrive(1, d, 0)
        arrive(1, d, 1)
        if d + 1 < pairs:
            arrive(0, d + 1, 1)
        compute(1, d)
        keep(d)
        if d > 0:
            relay(d - 1)
        pass_on(d)
    relay(pairs - 1)

    total = acc[z]
    for d, r in peers:
        row = row_of(d, r)
        remote(ret.at[row], ret.at[row], rs.at[row], rr.at[row], along(row)).wait_recv()
        total += ret[row].astype(jnp.float32)
    squares = jnp.sum(total * total, axis=1, keepdims=True)
    sq[...] = jnp.broadcast_to(squares, sq.shape)
    share = remote(sq, sqr, qs, qr, twin)
    share.start()
    own_gain.wait()
    share.wait()
    mean = (squares + sqr[:, :1]) / (half * 2)
    out[...] = (total * lax.rsqrt(mean + norm_eps) * gain[...]).astype(jnp.bfloat16)
    for copy in started:
        copy.wait_send()


def shards(hidden_state, expert_ids, route_weight, gate_matrix, up_matrix, down_matrix, norm_gain):
    tok, top = expert_ids.shape
    half = hidden_state.shape[1]
    hid = gate_matrix.shape[2]
    n = lax.axis_size("ep")
    if 2 * tok * top // n < tok or lax.axis_size("tp") != 2 or n % 4:
        return slotted(
            hidden_state, expert_ids, route_weight, gate_matrix, up_matrix, down_matrix, norm_gain
        )
    nx = 2
    nz = n // nx
    bf16, f32 = jnp.bfloat16, jnp.float32
    vmem = pl.BlockSpec(memory_space=pltpu.VMEM)
    hbm = pl.BlockSpec(memory_space=pl.ANY)
    dma = pltpu.SemaphoreType.DMA
    return pl.pallas_call(
        functools.partial(kernel, nz, nx),
        out_shape=jax.ShapeDtypeStruct((tok, half), bf16),
        in_specs=[hbm] * 7,
        out_specs=vmem,
        scratch_shapes=[
            pltpu.VMEM((nz, top, tok), jnp.int32),
            pltpu.VMEM((nz, top, tok), f32),
            pltpu.VMEM((1, half), f32),
            pltpu.VMEM((2, n, tok, half), bf16),
            pltpu.VMEM((2 * half, hid), bf16),
            pltpu.VMEM((2 * half, hid), bf16),
            pltpu.VMEM((hid, 2 * half), bf16),
            pltpu.VMEM((2 * tok, hid), bf16),
            pltpu.VMEM((nz, 2 * tok, half), bf16),
            pltpu.VMEM((nz, 2 * tok, half), bf16),
            pltpu.VMEM((nz, tok, half), f32),
            pltpu.VMEM((nz, tok, half), bf16),
            pltpu.VMEM((nz, tok, half), bf16),
            pltpu.VMEM((nz, tok, half), bf16),
            pltpu.VMEM((nz, tok, half), bf16),
            pltpu.VMEM((tok, 128), f32),
            pltpu.VMEM((tok, 128), f32),
            dma((3,)),
            dma((4,)),
            dma((nz,)),
            dma((n,)),
            dma((nz,)),
            dma((n,)),
            dma((n,)),
            dma((2, nz)),
            dma((2, nz)),
            dma((nz,)),
            dma((nz,)),
            dma((nz,)),
            dma((nz,)),
            dma((nz,)),
            dma((nz,)),
            dma,
            dma,
        ],
        compiler_params=pltpu.CompilerParams(
            collective_id=0, has_side_effects=True, vmem_limit_bytes=60 * 1024 * 1024
        ),
    )(
        expert_ids.T, route_weight.T, hidden_state, gate_matrix, up_matrix, down_matrix,
        norm_gain.reshape(1, half),
    )


def solution(mesh):
    placed = (
        P(("grp", "ep"), "tp"),
        P(("grp", "ep"), None),
        P(("grp", "ep"), None),
        P("ep", None, "tp"),
        P("ep", None, "tp"),
        P("ep", "tp", None),
        P("tp"),
    )
    return jax.shard_map(
        shards, mesh=mesh, in_specs=placed, out_specs=P(("grp", "ep"), "tp"), check_vma=False
    )
```

time: 40 us -> 40.3 us (level); the launches traced: 39.2 us -> 40.2 us
  Pallas kernels: 32.3 us -> 38.7 us
  local copies, waits for them, and re-layouts: 6.87 us -> 1.47 us
    pallas_call x1, Pallas kernels: 32.3 us -> 38.7 us  [shards(): pl.pallas_call(functools.partial(kernel, nz, nx), out_shape=jax.ShapeDtyp...]
    unnamed x11 -> x1, local copies, waits for them, and re-layouts: 6.87 us -> 1.47 us
where the time goes in v2:
time: 40.3 us; the launch traced here: 40.2 us
  Pallas kernels  38.7 us (96%)
  local copies, waits for them, and re-layouts  1.47 us (4%)
    pallas_call x1, Pallas kernels, shards(): pl.pallas_call(functools.partial(kernel, nz, nx), out_shape=jax.ShapeDtyp...  38.7 us
    unnamed x1, local copies, waits for them, and re-layouts  1.47 us

profile of v2, /device:TPU:0, one launch (start us, length us, event | category | flops | bytes accessed | tf_op | source)
XLA Modules:
  0.0 40.2 jit_solution(12944657520927595286)
XLA Ops:
  0.0 38.7 %shard_map.73 = bf16[64,512]{1,0:T(8,128)(2,1)} custom-call(s32[4,64]{1,0:T(4,128)} %bitcast.3, f32[4,64]{1,0:T(4,128)} %bitcast.4, bf16[64,512]{1,0:T(8,128)(2,1)} %h_hbm.1, bf16[1,1024,1024]{2,1,0:T(8,128)(2,1)} %g_hbm.1, bf16[1,1024,1024]{2,1,0:T(8,128)(2,1)} %u_hbm.1, bf16[1,1024,1024]{2,1,0:T(8,128)(2,1)} %d_hbm.1, f32[1,512]{1,0:T(1,128)} %bitcast.5), custom_call_target="tpu_custom_call" | custom-call | tf_op jit(solution)/shard_map/pallas_call | solution.py:299
  38.7 1.5 %copy.9 = bf16[64,512]{1,0:T(8,128)(2,1)} copy(bf16[64,512]{1,0:T(8,128)(2,1)} %shard_map.73) | data formatting | bytes 131072

commit v3 on v2

--- a/solution.py
+++ b/solution.py
@@ -70,8 +70,8 @@
 
 def kernel(
     nz, nx, ids_hbm, rw_hbm, h_hbm, g_hbm, u_hbm, d_hbm, gain_hbm, out,
-    ids, rw, gain, xs, gw, uw, dw, act, psend, precv, acc, ys, yx, zs, ret, sq, sqr,
-    wsem, osem, gs, gr, fs, ps, pr, ns, nr, ds, dr, us, ur, rs, rr, qs, qr,
+    ids, rw, gain, xs, gw, uw, dw, act, psend, precv, ys, ret, sq, sqr,
+    wsem, osem, gs, gr, fs, ps, pr, ds, dr, rs, rr, qs, qr,
 ):
     tok, half = out.shape
     hid = gw.shape[1]
@@ -89,8 +89,8 @@
         return copy
 
     own = local(h_hbm, xs.at[c, mine], osem.at[0])
-    own_ids = local(ids_hbm, ids.at[z], osem.at[1])
-    own_rw = local(rw_hbm, rw.at[z], osem.at[2])
+    own_ids = local(ids_hbm, ids, osem.at[1])
+    own_rw = local(rw_hbm, rw, osem.at[2])
     weights = [
         local(g_hbm.at[0], gw, wsem.at[0]),
         local(u_hbm.at[0], uw, wsem.at[1]),
@@ -108,18 +108,13 @@
     peers = [spot for spot in spots if far(*spot)]
 
     barrier = pltpu.get_barrier_semaphore()
-    for d, r in peers:
+    for k in range(1, nz * nx):
         pl.semaphore_signal(
-            barrier, inc=1, device_id={"ep": row_of(d, r) * nx + x}, device_id_type=MESH
+            barrier, inc=1, device_id={"ep": (me + k) % (nz * nx)}, device_id_type=MESH
         )
-    pl.semaphore_signal(
-        barrier, inc=1, device_id={"ep": z * nx + beside}, device_id_type=MESH
-    )
     pl.semaphore_signal(barrier, inc=1, device_id={"tp": other}, device_id_type=MESH)
     own.wait()
-    own_ids.wait()
-    own_rw.wait()
-    pl.semaphore_wait(barrier, nz + 1)
+    pl.semaphore_wait(barrier, nz * nx)
 
     def remote(src, dst, send, recv, where):
         return pltpu.make_async_remote_copy(
@@ -146,11 +141,6 @@
         row = row_of(d, r)
         send(block, block, gs.at[row], gr.at[mine], along(row))
     send(block, block, ps.at[mine], pr.at[mine], twin)
-    for d, r in peers:
-        row = row_of(d, r)
-        send(ids.at[z], ids.at[z], ns.at[0, row], nr.at[0, z], along(row))
-        send(rw.at[z], rw.at[z], ns.at[1, row], nr.at[1, z], along(row))
-
     def arrive(j, d, r):
         if j == 0 and not far(d, r):
             return
@@ -196,79 +186,64 @@
         kept[q] = swap
         part = jnp.dot(act[...], dw[:, ours], preferred_element_type=jnp.float32)
         part = part.astype(jnp.bfloat16).reshape(2, tok, half)
-        lower = 2 * ((z // 2 + d) % pairs)
-        if j == 0:
-            acc[pl.ds(lower, 2)] = part.astype(jnp.float32)
-        else:
-            ys[pl.ds(lower, 2)] = part
+        ys[pl.ds(base, 2)] = part
 
     eye = lax.broadcasted_iota(jnp.int32, (tok, tok), 0) == lax.broadcasted_iota(
         jnp.int32, (tok, tok), 1
     )
 
-    def weight_of(row, chip):
+    def weight_of(chip):
         line = jnp.zeros((1, tok), jnp.float32)
-        for k in range(ids.shape[1]):
-            line += jnp.where(ids[row, k : k + 1] == chip, rw[row, k : k + 1], 0.0)
+        for k in range(ids.shape[0]):
+            line += jnp.where(ids[k : k + 1] == chip, rw[k : k + 1], 0.0)
         return jnp.sum(jnp.where(eye, line, 0.0), axis=1, keepdims=True)
 
-    def keep(d):
-        q = 2 * d
+    def give_back(j, d):
+        q = 2 * d + j
         kept[q].wait()
-        for r in range(2):
-            row = row_of(d, r)
-            if far(d, r):
-                for i, ref in enumerate((ids, rw)):
-                    remote(
-                        ref.at[row], ref.at[row], ns.at[i, row], nr.at[i, row], along(row)
-                    ).wait_recv()
-            got = precv[q, pl.ds(pl.multiple_of(row % 2 * tok, tok), tok)]
-            done = (acc[row] + got.astype(jnp.float32)).astype(jnp.bfloat16)
-            acc[row] = done.astype(jnp.float32) * weight_of(row, me)
-
-    def pass_on(d):
-        q = 2 * d + 1
-        kept[q].wait()
+        column = (x + j) % nx
         for r in (1, 0):
             row = row_of(d, r)
+            slot = column * nz + row
             got = precv[q, pl.ds(pl.multiple_of(row % 2 * tok, tok), tok)]
-            done = ys[row].astype(jnp.float32) + got.astype(jnp.float32)
-            ys[row] = done.astype(jnp.bfloat16)
-            send(ys.at[row], yx.at[row], us.at[row], ur.at[row], across)
-
-    def relay(d):
-        for r in (1, 0):
-            row = row_of(d, r)
-            weight = weight_of(row, z * nx + beside)
-            remote(yx.at[row], yx.at[row], us.at[row], ur.at[row], across).wait_recv()
-            both = acc[row] + weight * yx[row].astype(jnp.float32)
-            if far(d, r):
-                zs[row] = both.astype(jnp.bfloat16)
-                send(zs.at[row], ret.at[z], rs.at[row], rr.at[z], along(row))
-            else:
-                acc[row] = both
+            done = ys[slot].astype(jnp.float32) + got.astype(jnp.float32)
+            ys[slot] = done.astype(jnp.bfloat16)
+            if j or far(d, r):
+                send(
+                    ys.at[slot], ret.at[mine], rs.at[slot], rr.at[mine],
+                    {"ep": row * nx + column},
+                )
 
     arrive(0, 0, 1)
-    for d in range(pairs):
-        if d > 0:
-            arrive(0, d, 0)
+    arrive(1, 0, 0)
+    compute(0, 0)
+    for d in range(1, pairs):
+        arrive(0, d, 1)
+        arrive(0, d, 0)
+    arrive(1, 0, 1)
+    give_back(0, 0)
+    for d in range(1, pairs):
         compute(0, d)
+    compute(1, 0)
+    for d in range(1, pairs):
+        give_back(0, d)
+    for d in range(1, pairs):
+        arrive(1, d, 1)
         arrive(1, d, 0)
-        arrive(1, d, 1)
-        if d + 1 < pairs:
-            arrive(0, d + 1, 1)
+    give_back(1, 0)
+    for d in range(1, pairs):
         compute(1, d)
-        keep(d)
-        if d > 0:
-            relay(d - 1)
-        pass_on(d)
-    relay(pairs - 1)
-
-    total = acc[z]
-    for d, r in peers:
-        row = row_of(d, r)
-        remote(ret.at[row], ret.at[row], rs.at[row], rr.at[row], along(row)).wait_recv()
-        total += ret[row].astype(jnp.float32)
+        give_back(1, d)
+
+    own_ids.wait()
+    own_rw.wait()
+    total = weight_of(me) * ys[mine].astype(jnp.float32)
+    for j, d, r in [(0, d, r) for d, r in peers] + [(1, d, r) for d, r in spots]:
+        column, row = (x + j) % nx, row_of(d, r)
+        slot = column * nz + row
+        weight = weight_of(row * nx + column)
+        remote(ret.at[slot], ret.at[slot], rs.at[slot], rr.at[slot], twin).wait_recv()
+        total += weight * ret[slot].astype(jnp.float32)
     squares = jnp.sum(total * total, axis=1, keepdims=True)
     sq[...] = jnp.broadcast_to(squares, sq.shape)
     share = remote(sq, sqr, qs, qr, twin)
@@ -294,16 +269,15 @@
     nz = n // nx
     bf16, f32 = jnp.bfloat16, jnp.float32
     vmem = pl.BlockSpec(memory_space=pltpu.VMEM)
-    hbm = pl.BlockSpec(memory_space=pl.ANY)
     dma = pltpu.SemaphoreType.DMA
     return pl.pallas_call(
         functools.partial(kernel, nz, nx),
         out_shape=jax.ShapeDtypeStruct((tok, half), bf16),
-        in_specs=[hbm] * 7,
+        in_specs=[pl.BlockSpec(memory_space=pl.ANY)] * 7,
         out_specs=vmem,
         scratch_shapes=[
-            pltpu.VMEM((nz, top, tok), jnp.int32),
-            pltpu.VMEM((nz, top, tok), f32),
+            pltpu.VMEM((top, tok), jnp.int32),
+            pltpu.VMEM((top, tok), f32),
             pltpu.VMEM((1, half), f32),
             pltpu.VMEM((2, n, tok, half), bf16),
             pltpu.VMEM((2 * half, hid), bf16),
@@ -312,11 +286,8 @@
             pltpu.VMEM((2 * tok, hid), bf16),
             pltpu.VMEM((nz, 2 * tok, half), bf16),
             pltpu.VMEM((nz, 2 * tok, half), bf16),
-            pltpu.VMEM((nz, tok, half), f32),
-            pltpu.VMEM((nz, tok, half), bf16),
-            pltpu.VMEM((nz, tok, half), bf16),
-            pltpu.VMEM((nz, tok, half), bf16),
-            pltpu.VMEM((nz, tok, half), bf16),
+            pltpu.VMEM((n, tok, half), bf16),
+            pltpu.VMEM((n, tok, half), bf16),
             pltpu.VMEM((tok, 128), f32),
             pltpu.VMEM((tok, 128), f32),
             dma((3,)),
@@ -326,14 +297,10 @@
             dma((nz,)),
             dma((n,)),
             dma((n,)),
-            dma((2, nz)),
-            dma((2, nz)),
             dma((nz,)),
             dma((nz,)),
-            dma((nz,)),
-            dma((nz,)),
-            dma((nz,)),
-            dma((nz,)),
+            dma((n,)),
+            dma((n,)),
             dma,
             dma,
         ],

time: 40.3 us -> 33.3 us (0.83)
  Pallas kernels: 38.7 us -> 31.7 us
    pallas_call x1, Pallas kernels: 38.7 us -> 31.7 us  [shards(): pl.pallas_call(functools.partial(kernel, nz, nx), out_shape=jax.ShapeDtyp...]
where the time goes in v3:
time: 33.3 us; the launch traced here: 33.2 us
  Pallas kernels  31.7 us (95%)
  local copies, waits for them, and re-layouts  1.47 us (4%)
    pallas_call x1, Pallas kernels, shards(): pl.pallas_call(functools.partial(kernel, nz, nx), out_shape=jax.ShapeDtyp...  31.7 us
    unnamed x1, local copies, waits for them, and re-layouts  1.47 us

profile of v3, /device:TPU:0, one launch (start us, length us, event | category | flops | bytes accessed | tf_op | source)
XLA Modules:
  0.0 33.2 jit_solution(6761285609091347538)
XLA Ops:
  0.0 31.7 %shard_map.73 = bf16[64,512]{1,0:T(8,128)(2,1)} custom-call(s32[4,64]{1,0:T(4,128)} %bitcast.3, f32[4,64]{1,0:T(4,128)} %bitcast.4, bf16[64,512]{1,0:T(8,128)(2,1)} %h_hbm.1, bf16[1,1024,1024]{2,1,0:T(8,128)(2,1)} %g_hbm.1, bf16[1,1024,1024]{2,1,0:T(8,128)(2,1)} %u_hbm.1, bf16[1,1024,1024]{2,1,0:T(8,128)(2,1)} %d_hbm.1, f32[1,512]{1,0:T(1,128)} %bitcast.5), custom_call_target="tpu_custom_call" | custom-call | tf_op jit(solution)/shard_map/pallas_call | solution.py:273
  31.7 1.5 %copy.9 = bf16[64,512]{1,0:T(8,128)(2,1)} copy(bf16[64,512]{1,0:T(8,128)(2,1)} %shard_map.73) | data formatting | bytes 131072

commit v4 on v3

--- a/solution.py
+++ b/solution.py
@@ -224,13 +224,13 @@
     give_back(0, 0)
     for d in range(1, pairs):
         compute(0, d)
+    for d in range(1, pairs):
+        give_back(0, d)
     compute(1, 0)
-    for d in range(1, pairs):
-        give_back(0, d)
+    give_back(1, 0)
     for d in range(1, pairs):
         arrive(1, d, 1)
         arrive(1, d, 0)
-    give_back(1, 0)
     for d in range(1, pairs):
         compute(1, d)
         give_back(1, d)

time: 33.3 us -> 32.8 us (0.985)
  Pallas kernels: 31.7 us -> 31.2 us
    pallas_call x1, Pallas kernels: 31.7 us -> 31.2 us  [shards(): pl.pallas_call(functools.partial(kernel, nz, nx), out_shape=jax.ShapeDtyp...]
where the time goes in v4:
time: 32.8 us; the launch traced here: 32.7 us
  Pallas kernels  31.2 us (95%)
  local copies, waits for them, and re-layouts  1.47 us (4%)
    pallas_call x1, Pallas kernels, shards(): pl.pallas_call(functools.partial(kernel, nz, nx), out_shape=jax.ShapeDtyp...  31.2 us
    unnamed x1, local copies, waits for them, and re-layouts  1.47 us

profile of v4, /device:TPU:0, one launch (start us, length us, event | category | flops | bytes accessed | tf_op | source)
XLA Modules:
  0.0 32.7 jit_solution(7533726862049239487)
XLA Ops:
  0.0 31.2 %shard_map.73 = bf16[64,512]{1,0:T(8,128)(2,1)} custom-call(s32[4,64]{1,0:T(4,128)} %bitcast.3, f32[4,64]{1,0:T(4,128)} %bitcast.4, bf16[64,512]{1,0:T(8,128)(2,1)} %h_hbm.1, bf16[1,1024,1024]{2,1,0:T(8,128)(2,1)} %g_hbm.1, bf16[1,1024,1024]{2,1,0:T(8,128)(2,1)} %u_hbm.1, bf16[1,1024,1024]{2,1,0:T(8,128)(2,1)} %d_hbm.1, f32[1,512]{1,0:T(1,128)} %bitcast.5), custom_call_target="tpu_custom_call" | custom-call | tf_op jit(solution)/shard_map/pallas_call | solution.py:273
  31.2 1.5 %copy.9 = bf16[64,512]{1,0:T(8,128)(2,1)} copy(bf16[64,512]{1,0:T(8,128)(2,1)} %shard_map.73) | data formatting | bytes 131072
